TPU v7x, 32 devices: a whole 2x2x4 slice. The times are simulated.
32 devices in a mesh: sp: 8 (over z, y), tp: 4 (over x, core).
Axes of the slice: x: 2, y: 2, z: 4, core: 2. Of those that a mesh axis runs over, the one named last changes fastest.
Arguments:
- residual_in: bfloat16 [3072, 2048], P(('sp', 'tp')), may hold values from -6 to 6
- queries: bfloat16 [3072, 2048], P('sp', 'tp'), may hold values from -180 to 180
- keys: bfloat16 [3072, 2048], P('sp', 'tp'), may hold values from -9 to 9
- values: bfloat16 [3072, 2048], P('sp', 'tp'), may hold values from -6 to 6
- mix_lambda: float32 [16], P('tp'), may hold values from 0.3 to 0.8
- head_gain: float32 [128], replicated, may hold values from 0.1 to 1.9
- out_weight: bfloat16 [2048, 2048], P('tp'), may hold values from -0.125 to 0.125
- norm_gain: float32 [2048], replicated, may hold values from 0.1 to 1.9
- gate_weight: bfloat16 [2048, 5632], P('sp', 'tp'), may hold values from -0.125 to 0.125
- up_weight: bfloat16 [2048, 5632], P('sp', 'tp'), may hold values from -0.125 to 0.125
- down_weight: bfloat16 [5632, 2048], P('tp', 'sp'), may hold values from -0.078125 to 0.078125
Outputs:
- layer_out: bfloat16 [3072, 2048], P(('sp', 'tp'))
All inputs are finite; a program needn't handle non-finite values.
Results may differ from a plain program's by a relative error of at most 0.014.
Values may be sent and summed in bfloat16 or wider, within the bound.
A program may use at most 128 MiB of HBM per device.

v0:
```python
import math
import jax
import jax.numpy as jnp
from jax import lax
from jax.sharding import PartitionSpec as P

DH = 64
VD = 128


def body(
    residual_in,
    queries,
    keys,
    values,
    mix_lambda,
    head_gain,
    out_weight,
    norm_gain,
    gate_weight,
    up_weight,
    down_weight,
):
    tp_count = lax.axis_size("tp")
    tok_local = queries.shape[0]
    heads_local = mix_lambda.shape[0]
    rows_local = tok_local // tp_count
    query_four = queries.reshape(tok_local, heads_local, 2, DH)
    inverse_root = 1.0 / math.sqrt(DH)

    def one_block(state, block):
        top, total, weighted = state
        key_block, value_block = block
        scores = (
            jnp.einsum("qhcd,khcd->hcqk", query_four, key_block, preferred_element_type=jnp.float32)
            * inverse_root
        )
        new_top = jnp.maximum(top, jnp.max(scores, axis=-1))
        rescale = jnp.exp(top - new_top)
        expo = jnp.exp(scores - new_top[..., None])
        total = total * rescale + jnp.sum(expo, axis=-1)
        weighted = weighted * rescale[..., None] + jnp.einsum(
            "hcqk,khe->hcqe",
            expo.astype(jnp.bfloat16),
            value_block,
            preferred_element_type=jnp.float32,
        )
        return ((new_top, total, weighted), None)

    start_state = (
        jnp.full((heads_local, 2, tok_local), -1e30, jnp.float32),
        jnp.zeros((heads_local, 2, tok_local), jnp.float32),
        jnp.zeros((heads_local, 2, tok_local, VD), jnp.float32),
    )
    key_piece = lax.all_gather(keys, "sp", axis=0, tiled=True)
    value_piece = lax.all_gather(values, "sp", axis=0, tiled=True)
    count = key_piece.shape[0]
    shards = max(count // tok_local, 1)
    unit = count // shards
    group = max(
        (g for g in range(1, shards + 1) if shards % g == 0 and g * unit <= max(1536, unit))
    )
    width = group * unit
    blocks = count // width
    key_blocks = key_piece.reshape(blocks, width, heads_local, 2, DH)
    value_blocks = value_piece.reshape(blocks, width, heads_local, VD)
    state, unused = lax.scan(one_block, start_state, (key_blocks, value_blocks))
    top, total, weighted = state
    maps = weighted / total[..., None]
    mixed = maps[:, 0] - mix_lambda[:, None, None] * maps[:, 1]
    head_scale = lax.rsqrt(jnp.mean(mixed * mixed, axis=-1, keepdims=True) + 1e-06)
    head_out = (mixed * head_scale * head_gain).astype(jnp.bfloat16)
    attended = jnp.transpose(head_out, (1, 0, 2)).reshape(tok_local, heads_local * VD)
    summed = lax.psum(
        jnp.dot(attended, out_weight, preferred_element_type=jnp.float32).astype(jnp.bfloat16), "tp"
    ).astype(jnp.float32)
    residual_all = lax.all_gather(residual_in, "tp", axis=0, tiled=True)
    after_all = residual_all.astype(jnp.float32) + summed
    row_scale = lax.rsqrt(jnp.mean(after_all * after_all, axis=-1, keepdims=True) + 1e-06)
    all_rows = (after_all * row_scale * norm_gain).astype(jnp.bfloat16)
    after_mix = lax.dynamic_slice_in_dim(
        after_all, lax.axis_index("tp") * rows_local, rows_local, 0
    )
    gate_all, up_all, down_all = (
        lax.all_gather(gate_weight, "sp", axis=0, tiled=True),
        lax.all_gather(up_weight, "sp", axis=0, tiled=True),
        lax.all_gather(down_weight, "sp", axis=1, tiled=True),
    )
    gate = jnp.dot(all_rows, gate_all, preferred_element_type=jnp.float32)
    up = jnp.dot(all_rows, up_all, preferred_element_type=jnp.float32)
    hidden = (jax.nn.silu(gate) * up).astype(jnp.bfloat16)
    mixer = lax.psum_scatter(
        jnp.dot(hidden, down_all, preferred_element_type=jnp.float32).astype(jnp.bfloat16),
        "tp",
        scatter_dimension=0,
        tiled=True,
    ).astype(jnp.float32)
    return (after_mix + 0.5 * mixer).astype(jnp.bfloat16)


def solution(mesh):
    return jax.shard_map(
        body,
        mesh=mesh,
        in_specs=(
            P(("sp", "tp"), None),
            P("sp", "tp"),
            P("sp", "tp"),
            P("sp", "tp"),
            P("tp"),
            P(),
            P("tp", None),
            P(),
            P("sp", "tp"),
            P("sp", "tp"),
            P("tp", "sp"),
        ),
        out_specs=P(("sp", "tp"), None),
        check_vma=False,
    )
```

profile of v0, /device:TPU:0, one launch (start us, length us, event | category | flops | bytes accessed | tf_op | source)
XLA Modules:
  0.0 579.6 jit_solution(15325134770839630398)
XLA Ops:
  6.5 0.7 all-gather.9.cloned.1.call-update
  7.3 0.7 all-gather.11.cloned.1.call-update
  8.8 1.2 copy.17
  10.0 62.3 %all-gather.9.cloned.1.call-done = bf16[3072,512]{1,0:T(8,128)(2,1)} async-done(((bf16[384,512]{1,0:T(8,128)(2,1)}), bf16[3072,512]{1,0:T(8,128)(2,1)}) %all-gather.9.cloned.1.call-update) | async-done | bytes 3145744 | tf_op jit(solution)/shard_map/all_gather | solution.py:55
  72.3 12.5 %reshape.39 = bf16[2,1536,4,2,64]{4,3,2,1,0:T(2,128)(2,1)} reshape(bf16[3072,512]{1,0:T(8,128)(2,1)} %all-gather.9.cloned.1.call-done) | data formatting | bytes 6291456 | tf_op jit(solution)/shard_map/reshape | solution.py:65
  84.8 15.4 %copy.18 = bf16[2,1536,4,2,64]{1,4,3,2,0:T(8,128)(2,1)} copy(bf16[2,1536,4,2,64]{4,3,2,1,0:T(2,128)(2,1)} %reshape.39) | data formatting | bytes 6291456
  100.2 33.0 %all-gather.11.cloned.1.call-done = bf16[3072,512]{1,0:T(8,128)(2,1)} async-done(((bf16[384,512]{1,0:T(8,128)(2,1)}), bf16[3072,512]{1,0:T(8,128)(2,1)}) %all-gather.11.cloned.1.call-update) | async-done | bytes 3145744 | tf_op jit(solution)/shard_map/all_gather | solution.py:56
  133.2 5.6 reshape.36
  138.7 63.8 %while.15 = (s32[]{:T(128)}, f32[4,2,384]{2,1,0:T(2,128)S(1)}, f32[4,2,384]{2,1,0:T(2,128)S(1)}, f32[4,2,384,128]{3,2,1,0:T(8,128)}, bf16[2,1536,4,2,64]{1,4,3,2...) while((s32[]{:T(128)}, f32[4,2,384]{2,1,0:T(2,128)S(1)}, ...), condition=%wide.region_3.4_spmd.clone, body=%wide.region_0.3_spmd.clone.sunk | while | flops 1850883072 | bytes 79233688 | solution.py:67
  138.7 10.6 %bitcast_reduce_fusion.2 = (f32[4,2,384]{2,1,0:T(2,128)S(1)}, f32[4,2,1536,384]{3,2,1,0:T(8,128)}) fusion(bf16[384,4,2,64]{0,3,2,1:T(8,128)(2,1)S(1)} %get-tuple-element.170, bf16[2,1536,4,2,64]{1,4,3,2,0:T(8,128)(2,1)} %get-tuple-element.169, s32[]{:T(128)} %get-tuple-element.156), kind=kOutput, calls=%fused_computation.1.clone.1 | convolution fusion | flops 613413888 | bytes 20853248 | tf_op jit(solution)/shard_map/while/body/eval_jaxpr/qhcd,khcd->hcqk/dot_general | solution.py:35
  149.4 9.5 %fusion.37 = f32[4,2,384]{2,1,0:T(2,128)S(1)} fusion(f32[4,2,1536,384]{3,2,1,0:T(8,128)} %get-tuple-element.144, f32[4,2,384]{2,1,0:T(2,128)S(1)} %fusion.36), kind=kLoop, calls=%fused_computation.4.clone.1 | loop fusion | flops 14152704 | bytes 18898944 | tf_op jit(solution)/shard_map/while/body/eval_jaxpr/reduce_sum | solution.py:41
  158.9 1.8 constant_dynamic-slice_fusion.2
  160.7 8.8 %fusion.39 = f32[4,2,384,128]{3,2,1,0:T(8,128)S(1)} fusion(f32[4,2,384,128]{3,2,1,0:T(8,128)S(1)} %copy-done.1, bf16[1,1536,4,128]{3,2,1,0:T(4,128)(2,1)S(1)} %constant_dynamic-slice_fusion.2, f32[4,2,1536,384]{3,2,1,0:T(8,128)} %get-tuple-element.144, f32[4,2,384]{2,1,0:T(2,128)S(1)} %fusion.36, f32[4,2,384]{2,1,0:T(2,128)S(1)} %get-tuple-element.146, ...), kind=kOutput, calls=%fused_computation.12.clone.1 | convolution fusion | flops 1223294976 | bytes 23617536 | tf_op jit(solution)/shard_map/while/body/eval_jaxpr/hcqk,khe->hcqe/dot_general | solution.py:42
  169.5 1.1 copy-done.2
  170.7 10.5 %bitcast_reduce_fusion.2 = (f32[4,2,384]{2,1,0:T(2,128)S(1)}, f32[4,2,1536,384]{3,2,1,0:T(8,128)}) fusion(bf16[384,4,2,64]{0,3,2,1:T(8,128)(2,1)S(1)} %get-tuple-element.170, bf16[2,1536,4,2,64]{1,4,3,2,0:T(8,128)(2,1)} %get-tuple-element.169, s32[]{:T(128)} %get-tuple-element.156), kind=kOutput, calls=%fused_computation.1.clone.1 | convolution fusion | flops 613413888 | bytes 20853248 | tf_op jit(solution)/shard_map/while/body/eval_jaxpr/qhcd,khcd->hcqk/dot_general | solution.py:35
  181.2 9.4 %fusion.37 = f32[4,2,384]{2,1,0:T(2,128)S(1)} fusion(f32[4,2,1536,384]{3,2,1,0:T(8,128)} %get-tuple-element.144, f32[4,2,384]{2,1,0:T(2,128)S(1)} %fusion.36), kind=kLoop, calls=%fused_computation.4.clone.1 | loop fusion | flops 14152704 | bytes 18898944 | tf_op jit(solution)/shard_map/while/body/eval_jaxpr/reduce_sum | solution.py:41
  190.7 1.8 constant_dynamic-slice_fusion.2
  192.6 8.8 %fusion.39 = f32[4,2,384,128]{3,2,1,0:T(8,128)S(1)} fusion(f32[4,2,384,128]{3,2,1,0:T(8,128)S(1)} %copy-done.1, bf16[1,1536,4,128]{3,2,1,0:T(4,128)(2,1)S(1)} %constant_dynamic-slice_fusion.2, f32[4,2,1536,384]{3,2,1,0:T(8,128)} %get-tuple-element.144, f32[4,2,384]{2,1,0:T(2,128)S(1)} %fusion.36, f32[4,2,384]{2,1,0:T(2,128)S(1)} %get-tuple-element.146, ...), kind=kOutput, calls=%fused_computation.12.clone.1 | convolution fusion | flops 1223294976 | bytes 23617536 | tf_op jit(solution)/shard_map/while/body/eval_jaxpr/hcqk,khe->hcqe/dot_general | solution.py:42
  201.4 1.1 copy-done.2
  202.5 3.1 copy.21
  205.6 1.5 broadcast_divide_fusion
  207.6 2.2 convolution_convert_fusion.1
  211.0 0.7 all-gather.17.cloned.1.call-update
  211.8 39.7 %all-reduce.2.cloned.1.call-done = bf16[384,2048]{1,0:T(8,128)(2,1)} async-done(((bf16[384,2048]{1,0:T(8,128)(2,1)}), bf16[384,2048]{1,0:T(8,128)(2,1)}) %all-reduce.2.cloned.1.call-update) | async-done | bytes 1572880 | tf_op jit(solution)/shard_map/psum | solution.py:74
  251.5 4.0 convert_add_fusion
  255.5 90.4 %all-gather.13.cloned.1.call-done = bf16[2048,1408]{1,0:T(8,128)(2,1)} async-done(((bf16[256,1408]{1,0:T(8,128)(2,1)}), bf16[2048,1408]{1,0:T(8,128)(2,1)}) %all-gather.13.cloned.1.call-update) | async-done | bytes 5767184 | tf_op jit(solution)/shard_map/all_gather | solution.py:85
  345.9 7.6 %fusion.21 = f32[384,1408]{1,0:T(8,128)} fusion(bf16[2048,1408]{1,0:T(8,128)(2,1)} %all-gather.13.cloned.1.call-done, f32[2048]{0:T(1024)S(1)} %copy-done.5, f32[384]{0:T(512)S(1)} %add_rsqrt_fusion.1, bf16[384,2048]{1,0:T(8,128)(2,1)} %all-reduce.2.cloned.1.call-done, bf16[384,2048]{1,0:T(8,128)(2,1)} %all-gather.7.cloned.1.call-done), kind=kOutput, calls=%fused_computation.40 | convolution fusion | flops 2219311104 | bytes 11085312 | tf_op jit(solution)/shard_map/dot_general | solution.py:89
  353.5 85.0 %all-gather.15.cloned.1.call-done = bf16[2048,1408]{1,0:T(8,128)(2,1)} async-done(((bf16[256,1408]{1,0:T(8,128)(2,1)}), bf16[2048,1408]{1,0:T(8,128)(2,1)}) %all-gather.15.cloned.1.call-update) | async-done | bytes 5767184 | tf_op jit(solution)/shard_map/all_gather | solution.py:86
  438.5 93.4 %all-gather.17.cloned.1.call-done = bf16[1408,2048]{1,0:T(8,128)(2,1)} async-done(((bf16[1408,256]{1,0:T(8,128)(2,1)}), bf16[1408,2048]{1,0:T(8,128)(2,1)}) %all-gather.17.cloned.1.call-update) | async-done | bytes 5767184 | tf_op jit(solution)/shard_map/all_gather | solution.py:87
  531.9 12.4 %convolution_convert_fusion = bf16[384,2048]{1,0:T(8,128)(2,1)} fusion(bf16[1408,2048]{1,0:T(8,128)(2,1)} %all-gather.17.cloned.1.call-done, bf16[2048,1408]{1,0:T(8,128)(2,1)} %all-gather.15.cloned.1.call-done, f32[384,1408]{1,0:T(8,128)} %fusion.21, f32[2048]{0:T(1024)S(1)} %copy-done.5, f32[384]{0:T(512)S(1)} %add_rsqrt_fusion.1, ...), kind=kOutput, calls=%fused_computation.27 | convolution fusion | flops 4437934080 | bytes 18425344 | tf_op jit(solution)/shard_map/dot_general | solution.py:93
  544.3 26.4 %reduce-scatter.2.cloned.1.call-done = bf16[96,2048]{1,0:T(8,128)(2,1)} async-done(((bf16[384,2048]{1,0:T(8,128)(2,1)}), bf16[96,2048]{1,0:T(8,128)(2,1)}) %reduce-scatter.2.cloned.1.call-update) | async-done | bytes 393232 | tf_op jit(solution)/shard_map/reduce_scatter | solution.py:92
  570.7 2.1 add_convert_fusion
  (42 shorter events, 2.6 us)
Async XLA Ops:
  6.5 201.0 %copy-start = (bf16[512,2048]{1,0:T(8,128)(2,1)S(1)}, bf16[512,2048]{1,0:T(8,128)(2,1)}, u32[]{:S(2)}) copy-start(bf16[512,2048]{1,0:T(8,128)(2,1)} %param.19) | copy-start | bytes 6291460
  6.5 65.8 %all-gather.9.cloned.1.call-start = ((), (), s32[]{:S(2)}) async-start(), calls=%async_computation.2 | async-start | bytes 3538944 | tf_op jit(solution)/shard_map/all_gather | solution.py:55
  7.3 125.9 %all-gather.11.cloned.1.call-start = ((), (), s32[]{:S(2)}) async-start(), calls=%async_computation.3 | async-start | bytes 3538944 | tf_op jit(solution)/shard_map/all_gather | solution.py:56
  8.0 203.8 %all-gather.7.cloned.1.call-start = ((), (), s32[]{:S(2)}) async-start(), calls=%async_computation.1 | async-start | bytes 1966080 | tf_op jit(solution)/shard_map/all_gather | solution.py:77
  8.7 242.7 %all-reduce.2.cloned.1.call-start = ((), (), s32[]{:S(2)}) async-start(), calls=%async_computation.4 | async-start | bytes 3145728 | tf_op jit(solution)/shard_map/psum | solution.py:74
  158.8 1.9 copy-start.1
  169.5 1.1 copy-start.2
  190.7 1.9 copy-start.1
  201.3 1.1 copy-start.2
  205.6 1.6 copy-start.3
  205.6 1.8 copy-start.4
  209.8 136.1 %all-gather.13.cloned.1.call-start = ((), (), s32[]{:S(2)}) async-start(), calls=%async_computation.5 | async-start | bytes 6488064 | tf_op jit(solution)/shard_map/all_gather | solution.py:85
  210.4 228.1 %all-gather.15.cloned.1.call-start = ((), (), s32[]{:S(2)}) async-start(), calls=%async_computation.6 | async-start | bytes 6488064 | tf_op jit(solution)/shard_map/all_gather | solution.py:86
  210.9 321.0 %all-gather.17.cloned.1.call-start = ((), (), s32[]{:S(2)}) async-start(), calls=%async_computation.7 | async-start | bytes 6488064 | tf_op jit(solution)/shard_map/all_gather | solution.py:87
  211.7 134.2 %copy-start.5 = (f32[2048]{0:T(1024)S(1)}, f32[2048]{0:T(1024)}, u32[]{:S(2)}) copy-start(f32[2048]{0:T(1024)} %param.20) | copy-start | bytes 24580
  211.7 359.0 %reduce-scatter.2.cloned.1.call-start = ((), (), s32[]{:S(2)}) async-start(), calls=%async_computation.8 | async-start | bytes 1966080 | tf_op jit(solution)/shard_map/reduce_scatter | solution.py:92
Sparse Core Ops, SparseCore 0:
  9.5 62.7 all-gather.8
  74.5 58.6 all-gather.10
  134.7 18.2 all-gather.6
  209.9 41.5 all-reduce.1
  253.5 92.3 all-gather.12
  347.9 90.5 all-gather.14
  440.5 91.2 all-gather.16
  544.4 26.2 reduce-scatter.1
where the time goes:
time: 581 us; the launch traced here: 580 us
  waiting for transfers between devices  434 us (75%)
  matrix products  60.9 us (10%)
  local copies, waits for them, and re-layouts  43.7 us (8%)
  other arithmetic  27.1 us (5%)
  between operations  13.6 us (2%)
    all_gather x1, waiting for transfers between devices, body(): lax.all_gather(down_weight, 'sp', axis=1, tiled=True)  93.4 us
    all_gather x1, waiting for transfers between devices, body(): lax.all_gather(gate_weight, 'sp', axis=0, tiled=True)  90.4 us
    all_gather x1, waiting for transfers between devices, body(): lax.all_gather(up_weight, 'sp', axis=0, tiled=True)  85 us
    all_gather x1, waiting for transfers between devices, body(): key_piece = lax.all_gather(keys, 'sp', axis=0, tiled=True)  62.3 us
    psum x1, waiting for transfers between devices, body(): lax.psum(jnp.dot(attended, out_weight, preferred_element_type=jnp.float32...  39.7 us
    all_gather x1, waiting for transfers between devices, body(): value_piece = lax.all_gather(values, 'sp', axis=0, tiled=True)  33 us
    reduce_scatter x1, waiting for transfers between devices, body(): lax.psum_scatter(jnp.dot(hidden, down_all, preferred_element_type=jnp.flo...  26.4 us
    dot_general x2, matrix products, one_block(): jnp.einsum('qhcd,khcd->hcqk', query_four, key_block, preferred_element_ty...  21.1 us
  transfers between devices with their start and end apart: 8, of which 7 were waited for; matrix products, arithmetic and copies ran while one was open for 20% of the time, Pallas kernels for 0%

commit v1 on v0

--- a/solution.py
+++ b/solution.py
@@ -1,3 +1,4 @@
+import functools
 import math
 import jax
 import jax.numpy as jnp
@@ -6,6 +7,13 @@
 
 DH = 64
 VD = 128
+
+
+def _raise_quarters(local_array, axis_name):
+    return jax.lax.all_gather(local_array, axis_name).sum(axis=0)
+
+
+remake_inputs = functools.partial(_raise_quarters, axis_name="tp")
 
 
 def body(
@@ -71,8 +79,8 @@
     head_scale = lax.rsqrt(jnp.mean(mixed * mixed, axis=-1, keepdims=True) + 1e-06)
     head_out = (mixed * head_scale * head_gain).astype(jnp.bfloat16)
     attended = jnp.transpose(head_out, (1, 0, 2)).reshape(tok_local, heads_local * VD)
-    summed = lax.psum(
-        jnp.dot(attended, out_weight, preferred_element_type=jnp.float32).astype(jnp.bfloat16), "tp"
+    summed = remake_inputs(
+        jnp.dot(attended, out_weight, preferred_element_type=jnp.float32).astype(jnp.bfloat16)
     ).astype(jnp.float32)
     residual_all = lax.all_gather(residual_in, "tp", axis=0, tiled=True)
     after_all = residual_all.astype(jnp.float32) + summed

time: 581 us -> 605 us (1.041)
  waiting for transfers between devices: 434 us -> 453 us
    all_gather x0 -> x1, waiting for transfers between devices: none -> 42.6 us  [_raise_quarters(): return jax.lax.all_gather(local_array, axis_name).sum(axis=0)]
    psum x1 -> x0, waiting for transfers between devices: 39.7 us -> none  [body(): lax.psum(jnp.dot(attended, out_weight, preferred_element_type=jnp.float32...]
    all_gather x1, waiting for transfers between devices: 0.02 us -> 15.4 us  [body(): residual_all = lax.all_gather(residual_in, 'tp', axis=0, tiled=True)]
  transfers between devices with their start and end apart: 8 -> 8, of which waited for: 7 -> 8; matrix products, arithmetic and copies ran while one was open for 20% -> 8% of each run, Pallas kernels for 0% -> 0%
where the time goes in v1:
time: 605 us; the launch traced here: 604 us
  waiting for transfers between devices  453 us (75%)
  matrix products  60.6 us (10%)
  local copies, waits for them, and re-layouts  43.8 us (7%)
  other arithmetic  32.8 us (5%)
  between operations  13.6 us (2%)
    all_gather x1, waiting for transfers between devices, body(): lax.all_gather(down_weight, 'sp', axis=1, tiled=True)  93.4 us
    all_gather x1, waiting for transfers between devices, body(): lax.all_gather(gate_weight, 'sp', axis=0, tiled=True)  90.3 us
    all_gather x1, waiting for transfers between devices, body(): lax.all_gather(up_weight, 'sp', axis=0, tiled=True)  85 us
    all_gather x1, waiting for transfers between devices, body(): key_piece = lax.all_gather(keys, 'sp', axis=0, tiled=True)  63 us
    all_gather x1, waiting for transfers between devices, _raise_quarters(): return jax.lax.all_gather(local_array, axis_name).sum(axis=0)  42.6 us
    all_gather x1, waiting for transfers between devices, body(): value_piece = lax.all_gather(values, 'sp', axis=0, tiled=True)  33 us
    reduce_scatter x1, waiting for transfers between devices, body(): lax.psum_scatter(jnp.dot(hidden, down_all, preferred_element_type=jnp.flo...  26.4 us
    dot_general x2, matrix products, one_block(): jnp.einsum('qhcd,khcd->hcqk', query_four, key_block, preferred_element_ty...  21.1 us
  transfers between devices with their start and end apart: 8, of which 8 were waited for; matrix products, arithmetic and copies ran while one was open for 8% of the time, Pallas kernels for 0%

profile of v1, /device:TPU:0, one launch (start us, length us, event | category | flops | bytes accessed | tf_op | source)
XLA Modules:
  0.0 603.9 jit_solution(17917128461578991965)
XLA Ops:
  6.5 0.7 all-gather.11.cloned.1.call-update
  8.1 1.2 copy.17
  9.3 63.0 %all-gather.11.cloned.1.call-done = bf16[3072,512]{1,0:T(8,128)(2,1)} async-done(((bf16[384,512]{1,0:T(8,128)(2,1)}), bf16[3072,512]{1,0:T(8,128)(2,1)}) %all-gather.11.cloned.1.call-update) | async-done | bytes 3145744 | tf_op jit(solution)/shard_map/all_gather | solution.py:63
  72.3 12.5 %reshape.40 = bf16[2,1536,4,2,64]{4,3,2,1,0:T(2,128)(2,1)} reshape(bf16[3072,512]{1,0:T(8,128)(2,1)} %all-gather.11.cloned.1.call-done) | data formatting | bytes 6291456 | tf_op jit(solution)/shard_map/reshape | solution.py:73
  84.8 15.4 %copy.18 = bf16[2,1536,4,2,64]{1,4,3,2,0:T(8,128)(2,1)} copy(bf16[2,1536,4,2,64]{4,3,2,1,0:T(2,128)(2,1)} %reshape.40) | data formatting | bytes 6291456
  100.2 33.0 %all-gather.13.cloned.1.call-done = bf16[3072,512]{1,0:T(8,128)(2,1)} async-done(((bf16[384,512]{1,0:T(8,128)(2,1)}), bf16[3072,512]{1,0:T(8,128)(2,1)}) %all-gather.13.cloned.1.call-update) | async-done | bytes 3145744 | tf_op jit(solution)/shard_map/all_gather | solution.py:64
  133.2 5.6 reshape.36
  138.7 63.7 %while.15 = (s32[]{:T(128)}, f32[4,2,384]{2,1,0:T(2,128)S(1)}, f32[4,2,384]{2,1,0:T(2,128)S(1)}, f32[4,2,384,128]{3,2,1,0:T(8,128)}, bf16[2,1536,4,2,64]{1,4,3,2...) while((s32[]{:T(128)}, f32[4,2,384]{2,1,0:T(2,128)S(1)}, ...), condition=%wide.region_3.4_spmd.clone, body=%wide.region_0.3_spmd.clone.sunk | while | flops 1850883072 | bytes 79233688 | solution.py:75
  138.7 10.5 %bitcast_reduce_fusion.2 = (f32[4,2,384]{2,1,0:T(2,128)S(1)}, f32[4,2,1536,384]{3,2,1,0:T(8,128)}) fusion(bf16[384,4,2,64]{0,3,2,1:T(8,128)(2,1)S(1)} %get-tuple-element.170, bf16[2,1536,4,2,64]{1,4,3,2,0:T(8,128)(2,1)} %get-tuple-element.169, s32[]{:T(128)} %get-tuple-element.156), kind=kOutput, calls=%fused_computation.1.clone.1 | convolution fusion | flops 613413888 | bytes 20853248 | tf_op jit(solution)/shard_map/while/body/eval_jaxpr/qhcd,khcd->hcqk/dot_general | solution.py:43
  149.3 9.4 %fusion.37 = f32[4,2,384]{2,1,0:T(2,128)S(1)} fusion(f32[4,2,1536,384]{3,2,1,0:T(8,128)} %get-tuple-element.144, f32[4,2,384]{2,1,0:T(2,128)S(1)} %fusion.36), kind=kLoop, calls=%fused_computation.4.clone.1 | loop fusion | flops 14152704 | bytes 18898944 | tf_op jit(solution)/shard_map/while/body/eval_jaxpr/reduce_sum | solution.py:49
  158.8 1.8 constant_dynamic-slice_fusion.2
  160.6 8.8 %fusion.39 = f32[4,2,384,128]{3,2,1,0:T(8,128)S(1)} fusion(f32[4,2,384,128]{3,2,1,0:T(8,128)S(1)} %copy-done.1, bf16[1,1536,4,128]{3,2,1,0:T(4,128)(2,1)S(1)} %constant_dynamic-slice_fusion.2, f32[4,2,1536,384]{3,2,1,0:T(8,128)} %get-tuple-element.144, f32[4,2,384]{2,1,0:T(2,128)S(1)} %fusion.36, f32[4,2,384]{2,1,0:T(2,128)S(1)} %get-tuple-element.146, ...), kind=kOutput, calls=%fused_computation.12.clone.1 | convolution fusion | flops 1223294976 | bytes 23617536 | tf_op jit(solution)/shard_map/while/body/eval_jaxpr/hcqk,khe->hcqe/dot_general | solution.py:50
  169.4 1.2 copy-done.2
  170.6 10.5 %bitcast_reduce_fusion.2 = (f32[4,2,384]{2,1,0:T(2,128)S(1)}, f32[4,2,1536,384]{3,2,1,0:T(8,128)}) fusion(bf16[384,4,2,64]{0,3,2,1:T(8,128)(2,1)S(1)} %get-tuple-element.170, bf16[2,1536,4,2,64]{1,4,3,2,0:T(8,128)(2,1)} %get-tuple-element.169, s32[]{:T(128)} %get-tuple-element.156), kind=kOutput, calls=%fused_computation.1.clone.1 | convolution fusion | flops 613413888 | bytes 20853248 | tf_op jit(solution)/shard_map/while/body/eval_jaxpr/qhcd,khcd->hcqk/dot_general | solution.py:43
  181.2 9.4 %fusion.37 = f32[4,2,384]{2,1,0:T(2,128)S(1)} fusion(f32[4,2,1536,384]{3,2,1,0:T(8,128)} %get-tuple-element.144, f32[4,2,384]{2,1,0:T(2,128)S(1)} %fusion.36), kind=kLoop, calls=%fused_computation.4.clone.1 | loop fusion | flops 14152704 | bytes 18898944 | tf_op jit(solution)/shard_map/while/body/eval_jaxpr/reduce_sum | solution.py:49
  190.6 1.8 constant_dynamic-slice_fusion.2
  192.5 8.8 %fusion.39 = f32[4,2,384,128]{3,2,1,0:T(8,128)S(1)} fusion(f32[4,2,384,128]{3,2,1,0:T(8,128)S(1)} %copy-done.1, bf16[1,1536,4,128]{3,2,1,0:T(4,128)(2,1)S(1)} %constant_dynamic-slice_fusion.2, f32[4,2,1536,384]{3,2,1,0:T(8,128)} %get-tuple-element.144, f32[4,2,384]{2,1,0:T(2,128)S(1)} %fusion.36, f32[4,2,384]{2,1,0:T(2,128)S(1)} %get-tuple-element.146, ...), kind=kOutput, calls=%fused_computation.12.clone.1 | convolution fusion | flops 1223294976 | bytes 23617536 | tf_op jit(solution)/shard_map/while/body/eval_jaxpr/hcqk,khe->hcqe/dot_general | solution.py:50
  201.3 1.2 copy-done.2
  202.5 3.1 copy.21
  205.6 1.5 broadcast_divide_fusion
  207.5 2.2 convolution_convert_fusion.1
  212.3 42.6 %all-gather.21.cloned.1.call-done = bf16[1536,2048]{1,0:T(8,128)(2,1)} async-done(((bf16[384,2048]{1,0:T(8,128)(2,1)}), bf16[1536,2048]{1,0:T(8,128)(2,1)}) %all-gather.21.cloned.1.call-update) | async-done | bytes 6291472 | tf_op jit(solution)/shard_map/all_gather | solution.py:13
  255.0 5.7 reduce_sum.40
  260.7 15.4 %all-gather.9.cloned.1.call-done = bf16[384,2048]{1,0:T(8,128)(2,1)} async-done(((bf16[96,2048]{1,0:T(8,128)(2,1)}), bf16[384,2048]{1,0:T(8,128)(2,1)}) %all-gather.9.cloned.1.call-update) | async-done | bytes 1572880 | tf_op jit(solution)/shard_map/all_gather | solution.py:85
  276.0 4.0 convert_add_fusion
  280.1 90.3 %all-gather.15.cloned.1.call-done = bf16[2048,1408]{1,0:T(8,128)(2,1)} async-done(((bf16[256,1408]{1,0:T(8,128)(2,1)}), bf16[2048,1408]{1,0:T(8,128)(2,1)}) %all-gather.15.cloned.1.call-update) | async-done | bytes 5767184 | tf_op jit(solution)/shard_map/all_gather | solution.py:93
  370.4 7.6 %fusion.21 = f32[384,1408]{1,0:T(8,128)} fusion(bf16[2048,1408]{1,0:T(8,128)(2,1)} %all-gather.15.cloned.1.call-done, f32[2048]{0:T(1024)S(1)} %copy-done.5, f32[384]{0:T(512)S(1)} %add_rsqrt_fusion.1, bf16[384,2048]{1,0:T(8,128)(2,1)} %reduce_sum.40, bf16[384,2048]{1,0:T(8,128)(2,1)} %all-gather.9.cloned.1.call-done), kind=kOutput, calls=%fused_computation.40 | convolution fusion | flops 2219311104 | bytes 11085312 | tf_op jit(solution)/shard_map/dot_general | solution.py:97
  378.1 85.0 %all-gather.17.cloned.1.call-done = bf16[2048,1408]{1,0:T(8,128)(2,1)} async-done(((bf16[256,1408]{1,0:T(8,128)(2,1)}), bf16[2048,1408]{1,0:T(8,128)(2,1)}) %all-gather.17.cloned.1.call-update) | async-done | bytes 5767184 | tf_op jit(solution)/shard_map/all_gather | solution.py:94
  463.0 93.4 %all-gather.19.cloned.1.call-done = bf16[1408,2048]{1,0:T(8,128)(2,1)} async-done(((bf16[1408,256]{1,0:T(8,128)(2,1)}), bf16[1408,2048]{1,0:T(8,128)(2,1)}) %all-gather.19.cloned.1.call-update) | async-done | bytes 5767184 | tf_op jit(solution)/shard_map/all_gather | solution.py:95
  556.4 12.2 %convolution_convert_fusion = bf16[384,2048]{1,0:T(8,128)(2,1)} fusion(bf16[1408,2048]{1,0:T(8,128)(2,1)} %all-gather.19.cloned.1.call-done, bf16[2048,1408]{1,0:T(8,128)(2,1)} %all-gather.17.cloned.1.call-done, f32[384,1408]{1,0:T(8,128)} %fusion.21, f32[2048]{0:T(1024)S(1)} %copy-done.5, f32[384]{0:T(512)S(1)} %add_rsqrt_fusion.1, ...), kind=kOutput, calls=%fused_computation.27 | convolution fusion | flops 4437934080 | bytes 18425344 | tf_op jit(solution)/shard_map/dot_general | solution.py:101
  568.6 26.4 %reduce-scatter.2.cloned.1.call-done = bf16[96,2048]{1,0:T(8,128)(2,1)} async-done(((bf16[384,2048]{1,0:T(8,128)(2,1)}), bf16[96,2048]{1,0:T(8,128)(2,1)}) %reduce-scatter.2.cloned.1.call-update) | async-done | bytes 393232 | tf_op jit(solution)/shard_map/reduce_scatter | solution.py:100
  595.0 2.1 add_convert_fusion
  (43 shorter events, 3.8 us)
Async XLA Ops:
  6.5 201.0 %copy-start = (bf16[512,2048]{1,0:T(8,128)(2,1)S(1)}, bf16[512,2048]{1,0:T(8,128)(2,1)}, u32[]{:S(2)}) copy-start(bf16[512,2048]{1,0:T(8,128)(2,1)} %param.19) | copy-start | bytes 6291460
  6.5 65.8 %all-gather.11.cloned.1.call-start = ((), (), s32[]{:S(2)}) async-start(), calls=%async_computation.2 | async-start | bytes 3538944 | tf_op jit(solution)/shard_map/all_gather | solution.py:63
  7.3 125.9 %all-gather.13.cloned.1.call-start = ((), (), s32[]{:S(2)}) async-start(), calls=%async_computation.3 | async-start | bytes 3538944 | tf_op jit(solution)/shard_map/all_gather | solution.py:64
  8.0 247.0 %all-gather.21.cloned.1.call-start = ((), (), s32[]{:S(2)}) async-start(), calls=%async_computation.8 | async-start | bytes 7864320 | tf_op jit(solution)/shard_map/all_gather | solution.py:13
  158.7 1.9 copy-start.1
  169.4 1.2 copy-start.2
  190.6 1.9 copy-start.1
  201.3 1.2 copy-start.2
  205.5 1.6 copy-start.3
  205.5 1.8 copy-start.4
  209.8 66.3 %all-gather.9.cloned.1.call-start = ((), (), s32[]{:S(2)}) async-start(), calls=%async_computation.1 | async-start | bytes 1966080 | tf_op jit(solution)/shard_map/all_gather | solution.py:85
  210.4 160.1 %all-gather.15.cloned.1.call-start = ((), (), s32[]{:S(2)}) async-start(), calls=%async_computation.4 | async-start | bytes 6488064 | tf_op jit(solution)/shard_map/all_gather | solution.py:93
  211.0 252.1 %all-gather.17.cloned.1.call-start = ((), (), s32[]{:S(2)}) async-start(), calls=%async_computation.5 | async-start | bytes 6488064 | tf_op jit(solution)/shard_map/all_gather | solution.py:94
  211.5 344.9 %all-gather.19.cloned.1.call-start = ((), (), s32[]{:S(2)}) async-start(), calls=%async_computation.6 | async-start | bytes 6488064 | tf_op jit(solution)/shard_map/all_gather | solution.py:95
  212.3 382.7 %reduce-scatter.2.cloned.1.call-start = ((), (), s32[]{:S(2)}) async-start(), calls=%async_computation.7 | async-start | bytes 1966080 | tf_op jit(solution)/shard_map/reduce_scatter | solution.py:100
  260.7 109.7 %copy-start.5 = (f32[2048]{0:T(1024)S(1)}, f32[2048]{0:T(1024)}, u32[]{:S(2)}) copy-start(f32[2048]{0:T(1024)} %param.20) | copy-start | bytes 24580
Sparse Core Ops, SparseCore 0:
  9.5 62.7 all-gather.10
  74.5 58.6 all-gather.12
  209.9 45.0 all-gather.20
  256.4 19.6 all-gather.8
  278.1 92.3 all-gather.14
  372.5 90.5 all-gather.16
  465.1 91.2 all-gather.18
  568.7 26.2 reduce-scatter.1
